TPU v7x, 128 devices: a whole 4x4x4 slice. The times are simulated.
128 devices in a mesh: kv: 32 (over z, y, core), tp: 4 (over x).
Axes of the slice: x: 4, y: 4, z: 4, core: 2. Of those that a mesh axis runs over, the one named last changes fastest.
Arguments:
- tokens: bfloat16 [512, 4, 4096], P('kv'), may hold values from -6 to 6
- norm_gain: bfloat16 [4096], replicated, may hold values from 0.099609375 to 1.8984375
- query_weight: bfloat16 [4096, 2048], P(None, 'tp'), may hold values from -0.09375 to 0.09375
- key_weight: bfloat16 [4096, 2048], P(None, 'tp'), may hold values from -0.09375 to 0.09375
- value_weight: bfloat16 [4096, 2048], P(None, 'tp'), may hold values from -0.09375 to 0.09375
- outgate_weight: bfloat16 [4096, 2048], P(None, 'tp'), may hold values from -0.09375 to 0.09375
- gate_weight: bfloat16 [4096, 32], replicated, may hold values from -0.09375 to 0.09375
- gate_bias: float32 [2, 16], replicated, may hold values from -1 to 4
- head_gain: bfloat16 [2048], P('tp'), may hold values from 0.099609375 to 1.8984375
- out_weight: bfloat16 [2048, 4096], P('tp', 'kv'), may hold values from -0.125 to 0.125
- state_c: float32 [512, 16, 128, 128], P('kv', 'tp'), may hold values from -3 to 3
- state_n: float32 [512, 16, 128], P('kv', 'tp'), may hold values from -3 to 3
- state_m: float32 [512, 16], P('kv', 'tp'), may hold values from -1 to 2
- prev_keys: bfloat16 [512, 16, 4, 128], P('kv', 'tp'), may hold values from -6 to 6
- prev_values: bfloat16 [512, 16, 4, 128], P('kv', 'tp'), may hold values from -6 to 6
- prev_gates: float32 [512, 16, 2, 4], P('kv', 'tp'), may hold values from -2 to 5
- accepted: int32 [512], P('kv'), may hold values from 0 to 4
Outputs:
- mixed: bfloat16 [512, 4, 4096], P(None, None, 'kv')
- carried_c: float32 [512, 16, 128, 128], P('kv', 'tp')
- carried_n: float32 [512, 16, 128], P('kv', 'tp')
- carried_m: float32 [512, 16], P('kv', 'tp')
- step_keys: bfloat16 [512, 16, 4, 128], P('kv', 'tp')
- step_values: bfloat16 [512, 16, 4, 128], P('kv', 'tp')
- step_gates: float32 [512, 16, 2, 4], P('kv', 'tp')
Inputs may be any that keep to these rules, and one draw needn't show every extreme that they name: accepted counts proposals of the last step, from none to all 4.
All inputs are finite; a program needn't handle non-finite values.
Results may differ from a plain program's by a relative error of at most 0.0075.
The roundings to bfloat16 on the way count: a program that leaves them out, or rounds other values in their place, can miss the bound.
Values may be sent and summed in bfloat16 or wider, within the bound.
No kernel may reach another device: no remote copies, remote signals or barrier semaphores. Data moves between devices by JAX's collectives and lax.ppermute only.
A program may use at most 128 MiB of HBM per device.

v0:
```python
import jax
import jax.numpy as jnp
from jax import lax
from jax.sharding import PartitionSpec as P

EPSILON = 1e-06
HIGHEST = lax.Precision.HIGHEST


def joined_along(tiles, dim):
    tiles = jnp.moveaxis(tiles, 0, dim)
    lengths = tiles.shape
    return tiles.reshape(*lengths[:dim], lengths[dim] * lengths[dim + 1], *lengths[dim + 2 :])


def from_everyone(x, axis):
    peers = lax.axis_size(axis)
    return lax.all_to_all(jnp.broadcast_to(x[None], (peers, *x.shape)), axis, 0, 0, tiled=True)


def collect(x, axis, dim):
    return joined_along(from_everyone(x, axis), dim)


def replay(state_c, state_n, state_m, keys_in, values_in, gates_in, accepted):
    proposals = keys_in.shape[2]
    scaled = keys_in.astype(jnp.float32) * keys_in.shape[3] ** (-0.5)
    values_f = values_in.astype(jnp.float32)
    igates = gates_in[:, :, 0, :]
    forget = jax.nn.log_sigmoid(gates_in[:, :, 1, :])
    position = jnp.arange(proposals, dtype=jnp.int32)
    within = position[None, None, :] < accepted[:, None, None]
    masked = jnp.where(within, forget, 0.0)
    summed = jnp.sum(masked, axis=-1)
    log_weight = jnp.where(
        within, summed[..., None] - jnp.cumsum(masked, axis=-1) + igates, -jnp.inf
    )
    carried_m = jnp.maximum(summed + state_m, jnp.max(log_weight, axis=-1))
    shrink = jnp.exp(summed + state_m - carried_m)
    weights = jnp.exp(log_weight - carried_m[..., None])
    carried_c = shrink[..., None, None] * state_c + jnp.einsum(
        "bhs,bhsv,bhsd->bhvd", weights, values_f, scaled, precision=HIGHEST
    )
    carried_n = shrink[..., None] * state_n + jnp.einsum(
        "bhs,bhsd->bhd", weights, scaled, precision=HIGHEST
    )
    return (carried_c, carried_n, carried_m)


def cell_block(state_c, state_n, state_m, queries, scaled, values_f, igates, forget):
    proposals = queries.shape[2]
    cumul = jnp.cumsum(forget, axis=-1)
    causal = jnp.tril(jnp.ones((proposals, proposals), dtype=bool))
    log_decay = jnp.where(
        causal, cumul[..., :, None] - cumul[..., None, :] + igates[..., None, :], -jnp.inf
    )
    carried = cumul + state_m[..., None]
    stable = jnp.maximum(carried, jnp.max(log_decay, axis=-1))
    scores = jnp.einsum("bhtd,bhsd->bhts", queries, scaled, precision=HIGHEST) * jnp.exp(
        log_decay - stable[..., None]
    )
    weight_state = jnp.exp(carried - stable)
    numer = weight_state[..., None] * jnp.einsum(
        "bhvd,bhtd->bhtv", state_c, queries, precision=HIGHEST
    )
    numer = numer + jnp.einsum("bhts,bhsv->bhtv", scores, values_f, precision=HIGHEST)
    denom = weight_state * jnp.einsum(
        "bhd,bhtd->bht", state_n, queries, precision=HIGHEST
    ) + jnp.sum(scores, axis=-1)
    return numer / jnp.maximum(jnp.abs(denom), jnp.exp(-stable))[..., None]


def gate_heads(hidden, gain, outgate):
    heads_count = hidden.shape[1]
    head_size = hidden.shape[3]
    normed = hidden * lax.rsqrt(jnp.mean(hidden * hidden, axis=-1, keepdims=True) + EPSILON)
    normed = normed * gain.astype(jnp.float32).reshape(heads_count, head_size)[None, :, None, :]
    rows_out = jnp.transpose(normed, (0, 2, 1, 3)).reshape(outgate.shape)
    return (rows_out * jax.nn.sigmoid(outgate.astype(jnp.float32))).astype(jnp.bfloat16)


def per_device(
    tokens,
    norm_gain,
    query_weight,
    key_weight,
    value_weight,
    outgate_weight,
    gate_weight,
    gate_bias,
    head_gain,
    out_weight,
    state_c,
    state_n,
    state_m,
    prev_keys,
    prev_values,
    prev_gates,
    accepted,
):
    seqs_local, proposals, features = tokens.shape
    heads_local = state_m.shape[1]
    head_size = state_n.shape[2]
    tokens_f = tokens.astype(jnp.float32)
    normed = tokens_f * lax.rsqrt(jnp.mean(tokens_f * tokens_f, axis=-1, keepdims=True) + EPSILON)
    normed = (normed * norm_gain.astype(jnp.float32)).astype(jnp.bfloat16)
    rows_in = normed.reshape(seqs_local * proposals, features)

    def project(matrix):
        return jnp.dot(rows_in, matrix, preferred_element_type=jnp.float32).astype(jnp.bfloat16)

    def by_head(array):
        return array.reshape(seqs_local, proposals, heads_local, head_size).transpose(0, 2, 1, 3)

    queries = project(query_weight)
    keys_new = project(key_weight)
    values_new = project(value_weight)
    outgate = project(outgate_weight)
    all_gates = (
        jnp.dot(rows_in, gate_weight, preferred_element_type=jnp.float32)
        + gate_bias.reshape(-1)[None, :]
    )
    heads_total = gate_weight.shape[1] // 2
    head_offset = lax.axis_index("tp") * heads_local
    igates = lax.dynamic_slice_in_dim(all_gates, head_offset, heads_local, 1)
    fgates = lax.dynamic_slice_in_dim(all_gates, heads_total + head_offset, heads_local, 1)
    igates = igates.reshape(seqs_local, proposals, heads_local).transpose(0, 2, 1)
    fgates = fgates.reshape(seqs_local, proposals, heads_local).transpose(0, 2, 1)
    step_gates = jnp.stack([igates, fgates], axis=2)
    carried_c, carried_n, carried_m = replay(
        state_c, state_n, state_m, prev_keys, prev_values, prev_gates, accepted
    )
    step_keys = by_head(keys_new)
    step_values = by_head(values_new)
    hidden = cell_block(
        carried_c,
        carried_n,
        carried_m,
        by_head(queries).astype(jnp.float32),
        step_keys.astype(jnp.float32) * head_size ** (-0.5),
        step_values.astype(jnp.float32),
        igates,
        jax.nn.log_sigmoid(fgates),
    )
    gated = gate_heads(hidden, head_gain, outgate)
    partial_out = jnp.dot(collect(gated, "kv", 0), out_weight, preferred_element_type=jnp.float32)
    summed = lax.psum(partial_out, "tp")
    mixed = summed.astype(jnp.bfloat16).reshape(-1, proposals, summed.shape[1])
    return (mixed, carried_c, carried_n, carried_m, step_keys, step_values, step_gates)


def solution(mesh):
    in_specs = (
        P("kv", None, None),
        P(),
        P(None, "tp"),
        P(None, "tp"),
        P(None, "tp"),
        P(None, "tp"),
        P(),
        P(),
        P("tp"),
        P("tp", "kv"),
        P("kv", "tp", None, None),
        P("kv", "tp", None),
        P("kv", "tp"),
        P("kv", "tp", None, None),
        P("kv", "tp", None, None),
        P("kv", "tp", None, None),
        P("kv"),
    )
    out_specs = (
        P(None, None, "kv"),
        P("kv", "tp", None, None),
        P("kv", "tp", None),
        P("kv", "tp"),
        P("kv", "tp", None, None),
        P("kv", "tp", None, None),
        P("kv", "tp", None, None),
    )
    return jax.shard_map(
        per_device, mesh=mesh, in_specs=in_specs, out_specs=out_specs, check_vma=False
    )
```

profile of v0, /device:TPU:0, one launch (start us, length us, event | category | flops | bytes accessed | tf_op | source)
XLA Modules:
  0.0 114.7 jit_solution(9230726068473415681)
XLA Ops:
  0.6 0.0 copy-start
  0.7 0.8 add.110
  1.5 0.7 iota_compare_fusion
  2.2 0.7 bitcast_convert_fusion
  2.9 0.8 copy.77
  3.6 1.4 %fusion.7 = f32[16,4]{1,0:T(8,128)S(1)} fusion(bf16[16,4,4096]{2,1,0:T(4,128)(2,1)} %param.17), kind=kLoop, calls=%fused_computation.16 | loop fusion | flops 786368 | bytes 524544 | tf_op jit(solution)/shard_map/reduce_sum | solution.py:105
  5.0 0.7 convert_element_type.41
  5.7 0.7 fusion.41
  6.5 0.1 copy.93
  6.6 0.1 copy.76
  6.7 1.4 %fusion.9 = bf16[16,4,4096]{2,1,0:T(4,128)(2,1)S(1)} fusion(bf16[16,4,4096]{2,1,0:T(4,128)(2,1)} %param.17, f32[4096]{0:T(1024)S(1)} %convert_element_type.41, f32[16,4]{1,0:T(8,128)S(1)} %add_rsqrt_fusion), kind=kLoop, calls=%fused_computation.18 | loop fusion | flops 1048576 | bytes 1065216 | tf_op jit(solution)/shard_map/convert_element_type | solution.py:106
  8.1 0.1 reshape.103
  8.2 0.3 convolution_add_fusion
  8.5 0.1 reshape.104
  8.6 0.1 reshape.105
  8.7 0.1 fusion.24
  8.8 0.1 fusion.39
  8.9 2.8 %reduce_window_sum.18 = f32[16,4,4]{2,1,0:T(4,128)S(1)} reduce-window(f32[16,4,4]{2,1,0:T(4,128)S(1)} %get-tuple-element.26, f32[]{:T(128)} %constant.13.clone.1), window={size=1x1x4 pad=0_0x0_0x3_0}, to_apply=%region_3.4 | reduce-window | flops 768 | bytes 2052 | tf_op jit(solution)/shard_map/jit(cumsum)/reduce_window_sum | solution.py:36
  11.7 2.7 %reduce_window_sum.17 = f32[16,4,4]{2,1,0:T(4,128)S(1)} reduce-window(f32[16,4,4]{2,1,0:T(4,128)S(1)} %fusion.24, f32[]{:T(128)} %constant.13.clone.1), window={size=1x1x4 pad=0_0x0_0x3_0}, to_apply=%region_1.2 | reduce-window | flops 768 | bytes 2052 | tf_op jit(solution)/shard_map/jit(cumsum)/reduce_window_sum | solution.py:52
  14.4 3.0 %convolution_convert_fusion.1 = bf16[64,512]{1,0:T(8,128)(2,1)S(1)} fusion(bf16[64,4096]{1,0:T(8,128)(2,1)S(1)} %reshape.103, bf16[4096,512]{1,0:T(8,128)(2,1)} %param.21), kind=kOutput, calls=%fused_computation.12 | convolution fusion | flops 268468224 | bytes 4784128 | tf_op jit(solution)/shard_map/dot_general | solution.py:110
  17.5 3.1 %convolution_convert_fusion.2 = bf16[64,512]{1,0:T(8,128)(2,1)S(1)} fusion(bf16[64,4096]{1,0:T(8,128)(2,1)S(1)} %reshape.103, bf16[4096,512]{1,0:T(8,128)(2,1)} %param.20), kind=kOutput, calls=%fused_computation.13 | convolution fusion | flops 268468224 | bytes 4784128 | tf_op jit(solution)/shard_map/dot_general | solution.py:110
  20.6 3.1 %convolution_convert_fusion.3 = bf16[64,512]{1,0:T(8,128)(2,1)S(1)} fusion(bf16[64,4096]{1,0:T(8,128)(2,1)S(1)} %reshape.103, bf16[4096,512]{1,0:T(8,128)(2,1)} %param.19), kind=kOutput, calls=%fused_computation.14 | convolution fusion | flops 268468224 | bytes 4784128 | tf_op jit(solution)/shard_map/dot_general | solution.py:110
  23.7 0.2 fusion.38
  23.9 0.2 fusion.16
  24.1 0.1 subtract_exponential_fusion.1
  24.2 0.6 fusion.13
  24.8 0.1 copy_bitcast_fusion
  24.9 0.0 copy-start.7
  24.9 0.0 copy-start.6
  24.9 0.1 multiply_add_fusion.1
  25.0 0.4 fusion.22
  25.4 0.5 fusion.42
  25.8 0.1 exponential_maximum_fusion
  25.9 0.1 fusion.29
  26.0 9.1 %multiply_add_fusion = f32[16,4,128,128]{3,2,1,0:T(8,128)S(1)} fusion(f32[16,4,128,128]{3,2,1,0:T(8,128)} %param.27, f32[16,4]{1,0:T(8,128)S(1)} %get-tuple-element.23, bf16[16,4,4,128]{3,2,1,0:T(4,128)(2,1)S(1)} %copy-done.4, bf16[16,4,4,128]{3,2,1,0:T(4,128)(2,1)S(1)} %copy-done.5, f32[16,4,4]{2,1,0:T(4,128)S(1)} %get-tuple-element.33), kind=kOutput, calls=%fused_computation | convolution fusion | flops 52559872 | bytes 8520960 | tf_op jit(solution)/shard_map/bhs,bhsv,bhsd->bhvd/dot_general | solution.py:41
  35.2 3.3 %fusion.23 = f32[16,4,4,128]{3,2,1,0:T(4,128)S(1)} fusion(f32[16,4,128,128]{3,2,1,0:T(8,128)S(1)} %multiply_add_fusion, bf16[16,4,4,128]{3,2,1,0:T(4,128)(2,1)S(1)} %reshape.106), kind=kOutput, calls=%fused_computation.43 | convolution fusion | flops 50331648 | bytes 4390912 | tf_op jit(solution)/shard_map/bhvd,bhtd->bhtv/dot_general | solution.py:63
  38.5 0.6 fusion.17
  39.2 0.3 multiply_multiply_fusion
  39.5 0.9 fusion.6
  40.4 1.6 %broadcast_in_dim.52 = bf16[32,64,512]{2,1,0:T(8,128)(2,1)} broadcast(bf16[64,512]{1,0:T(8,128)(2,1)S(1)} %fusion.6), dimensions={1,2} | broadcast | bytes 2162688 | tf_op jit(solution)/shard_map/broadcast_in_dim | solution.py:18
  42.0 8.4 %all-to-all-start = ((bf16[32,64,512]{2,1,0:T(8,128)(2,1)}), bf16[32,64,512]{2,1,0:T(8,128)(2,1)S(1)}, u32[]{:S(2)}, u32[]{:S(2)}) async-start(bf16[32,64,512]{2,1,0:T(8,128)(2,1)} %broadcast_in_dim.52), calls=%async_computation | async-start | bytes 4194304 | tf_op jit(solution)/shard_map/all_to_all | solution.py:18
  50.4 0.7 copy.87
  51.1 0.1 copy.85
  51.2 0.1 copy.86
  51.3 0.6 pad_maximum_fusion
  51.9 28.6 %all-to-all-done = bf16[32,64,512]{2,1,0:T(8,128)(2,1)S(1)} async-done(((bf16[32,64,512]{2,1,0:T(8,128)(2,1)}), bf16[32,64,512]{2,1,0:T(8,128)(2,1)S(1)}, u32[]{:S(2)}, u32[]{:S(2)}) %all-to-all-start) | async-done | bytes 2097184 | tf_op jit(solution)/shard_map/all_to_all | solution.py:18
  80.5 0.7 fusion.43
  81.2 33.5 %all-reduce.1 = bf16[2048,128]{1,0:T(8,128)(2,1)} all-reduce(f32[2048,128]{1,0:T(8,128)S(1)} %fusion.43), channel_id=1, replica_groups=mesh['kv'=32,'tp'=4] {'tp'}, use_global_device_ids=true, to_apply=%region_8.9 | all-reduce | flops 262144 | bytes 1572864 | tf_op jit(solution)/shard_map/psum | solution.py:147
  (28 shorter events, 0.2 us)
Async XLA Ops:
  0.6 7.6 %copy-start = (bf16[4096,32]{0,1:T(8,128)(2,1)S(1)}, bf16[4096,32]{0,1:T(8,128)(2,1)}, u32[]{:S(2)}) copy-start(bf16[4096,32]{0,1:T(8,128)(2,1)} %param.23) | copy-start | bytes 786436
  17.5 6.7 %copy-start.4 = (bf16[16,4,4,128]{3,2,1,0:T(4,128)(2,1)S(1)}, bf16[16,4,4,128]{3,2,1,0:T(4,128)(2,1)}, u32[]{:S(2)}) copy-start(bf16[16,4,4,128]{3,2,1,0:T(4,128)(2,1)} %param.30) | copy-start | bytes 196612
  20.6 4.3 %copy-start.8 = (f32[16,4,128]{2,1,0:T(4,128)S(1)}, f32[16,4,128]{2,1,0:T(4,128)}, u32[]{:S(2)}) copy-start(f32[16,4,128]{2,1,0:T(4,128)} %param.28) | copy-start | bytes 98308
  20.6 5.4 %copy-start.5 = (bf16[16,4,4,128]{3,2,1,0:T(4,128)(2,1)S(1)}, bf16[16,4,4,128]{3,2,1,0:T(4,128)(2,1)}, u32[]{:S(2)}) copy-start(bf16[16,4,4,128]{3,2,1,0:T(4,128)(2,1)} %param.31) | copy-start | bytes 196612
  24.9 10.3 %copy-start.7 = (bf16[16,4,4,128]{3,2,1,0:T(4,128)(2,1)}, bf16[16,4,4,128]{3,2,1,0:T(4,128)(2,1)S(1)}, u32[]{:S(2)}) copy-start(bf16[16,4,4,128]{3,2,1,0:T(4,128)(2,1)S(1)} %get-tuple-element.40) | copy-start | bytes 196612
  24.9 13.7 %copy-start.6 = (bf16[16,4,4,128]{3,2,1,0:T(4,128)(2,1)}, bf16[16,4,4,128]{3,2,1,0:T(4,128)(2,1)S(1)}, u32[]{:S(2)}) copy-start(bf16[16,4,4,128]{3,2,1,0:T(4,128)(2,1)S(1)} %get-tuple-element.39) | copy-start | bytes 196612
  25.0 0.8 copy-start.9
  35.2 5.2 %copy-start.1 = (f32[16,4,128,128]{3,2,1,0:T(8,128)}, f32[16,4,128,128]{3,2,1,0:T(8,128)S(1)}, u32[]{:S(2)}) copy-start(f32[16,4,128,128]{3,2,1,0:T(8,128)S(1)} %multiply_add_fusion) | copy-start | bytes 12582916
  35.2 4.3 %copy-start.2 = (bf16[4096,512]{1,0:T(8,128)(2,1)S(1)}, bf16[4096,512]{1,0:T(8,128)(2,1)}, u32[]{:S(2)}) copy-start(bf16[4096,512]{1,0:T(8,128)(2,1)} %param.22) | copy-start | bytes 12582916
  40.4 40.1 %copy-start.3 = (bf16[512,128]{1,0:T(8,128)(2,1)S(1)}, bf16[512,128]{1,0:T(8,128)(2,1)}, u32[]{:S(2)}) copy-start(bf16[512,128]{1,0:T(8,128)(2,1)} %param.26) | copy-start | bytes 393220
  42.0 38.5 %all-to-all-start = ((bf16[32,64,512]{2,1,0:T(8,128)(2,1)}), bf16[32,64,512]{2,1,0:T(8,128)(2,1)S(1)}, u32[]{:S(2)}, u32[]{:S(2)}) async-start(bf16[32,64,512]{2,1,0:T(8,128)(2,1)} %broadcast_in_dim.52), calls=%async_computation | async-start | bytes 4194304 | tf_op jit(solution)/shard_map/all_to_all | solution.py:18
where the time goes:
time: 115 us
  blocking collectives  33.5 us (29%)
  waiting for transfers between devices  28.6 us (25%)
  matrix products  25.4 us (22%)
  other arithmetic  12.3 us (11%)
  starting transfers between devices  8.44 us (7%)
  local copies, waits for them, and re-layouts  5.47 us (5%)
    psum x1, blocking collectives, per_device(): summed = lax.psum(partial_out, 'tp')  33.5 us
    all_to_all x1, waiting for transfers between devices, from_everyone(): lax.all_to_all(jnp.broadcast_to(x[None], (peers, *x.shape)), axis, 0, 0,...  28.6 us
    dot_general x4, matrix products, project(): jnp.dot(rows_in, matrix, preferred_element_type=jnp.float32)  9.99 us
    dot_general x1, matrix products, replay(): jnp.einsum('bhs,bhsv,bhsd->bhvd', weights, values_f, scaled, precision=HI...  9.09 us
    all_to_all x1, starting transfers between devices, from_everyone(): lax.all_to_all(jnp.broadcast_to(x[None], (peers, *x.shape)), axis, 0, 0,...  8.44 us
    dot_general x1, matrix products, cell_block(): jnp.einsum('bhvd,bhtd->bhtv', state_c, queries, precision=HIGHEST)  3.35 us
    another operation x1, other arithmetic, replay(): jnp.cumsum(masked, axis=-1)  2.76 us
    another operation x1, other arithmetic, cell_block(): cumul = jnp.cumsum(forget, axis=-1)  2.75 us
  transfers between devices with their start and end apart: 1, of which 1 were waited for; matrix products, arithmetic and copies ran while one was open for 1% of the time, Pallas kernels for 0%

commit v1 on v0

--- a/solution.py
+++ b/solution.py
@@ -144,7 +144,9 @@
     )
     gated = gate_heads(hidden, head_gain, outgate)
     partial_out = jnp.dot(collect(gated, "kv", 0), out_weight, preferred_element_type=jnp.float32)
-    summed = lax.psum(partial_out, "tp")
+    summed = partial_out
+    for hop in (1, 2):
+        summed = summed + lax.ppermute(summed, "tp", [(dev, dev ^ hop) for dev in range(4)])
     mixed = summed.astype(jnp.bfloat16).reshape(-1, proposals, summed.shape[1])
     return (mixed, carried_c, carried_n, carried_m, step_keys, step_values, step_gates)
 

time: 115 us -> 131 us (1.14)
  waiting for transfers between devices: 28.6 us -> 45 us
  starting transfers between devices: 8.44 us -> 4.67 us
  blocking collectives: 33.5 us -> 36.7 us
  local copies, waits for them, and re-layouts: 5.47 us -> 4.11 us
    ppermute x0 -> x2, waiting for transfers between devices: none -> 45 us  [per_device(): lax.ppermute(summed, 'tp', [(dev, dev ^ hop) for dev in range(4)])]
    all_to_all x0 -> x1, blocking collectives: none -> 36.7 us  [from_everyone(): lax.all_to_all(jnp.broadcast_to(x[None], (peers, *x.shape)), axis, 0, 0,...]
    psum x1 -> x0, blocking collectives: 33.5 us -> none  [per_device(): summed = lax.psum(partial_out, 'tp')]
    all_to_all x1 -> x0, waiting for transfers between devices: 28.6 us -> none  [from_everyone(): lax.all_to_all(jnp.broadcast_to(x[None], (peers, *x.shape)), axis, 0, 0,...]
    all_to_all x1 -> x0, starting transfers between devices: 8.44 us -> none  [from_everyone(): lax.all_to_all(jnp.broadcast_to(x[None], (peers, *x.shape)), axis, 0, 0,...]
    ppermute x0 -> x2, starting transfers between devices: none -> 4.67 us  [per_device(): lax.ppermute(summed, 'tp', [(dev, dev ^ hop) for dev in range(4)])]
    broadcast_in_dim x1, local copies, waits for them, and re-layouts: 1.59 us -> 0.23 us  [from_everyone(): jnp.broadcast_to(x[None], (peers, *x.shape))]
  transfers between devices with their start and end apart: 1 -> 2, of which waited for: 1 -> 2; matrix products, arithmetic and copies ran while one was open for 1% -> 1% of each run, Pallas kernels for 0% -> 0%
where the time goes in v1:
time: 131 us; the launch traced here: 130 us
  waiting for transfers between devices  45 us (34%)
  blocking collectives  36.7 us (28%)
  matrix products  25.4 us (19%)
  other arithmetic  13.3 us (10%)
  starting transfers between devices  4.67 us (4%)
  local copies, waits for them, and re-layouts  4.11 us (3%)
    ppermute x2, waiting for transfers between devices, per_device(): lax.ppermute(summed, 'tp', [(dev, dev ^ hop) for dev in range(4)])  45 us
    all_to_all x1, blocking collectives, from_everyone(): lax.all_to_all(jnp.broadcast_to(x[None], (peers, *x.shape)), axis, 0, 0,...  36.7 us
    dot_general x4, matrix products, project(): jnp.dot(rows_in, matrix, preferred_element_type=jnp.float32)  9.99 us
    dot_general x1, matrix products, replay(): jnp.einsum('bhs,bhsv,bhsd->bhvd', weights, values_f, scaled, precision=HI...  9.09 us
    ppermute x2, starting transfers between devices, per_device(): lax.ppermute(summed, 'tp', [(dev, dev ^ hop) for dev in range(4)])  4.67 us
    dot_general x1, matrix products, cell_block(): jnp.einsum('bhvd,bhtd->bhtv', state_c, queries, precision=HIGHEST)  3.35 us
    another operation x1, other arithmetic, replay(): jnp.cumsum(masked, axis=-1)  2.76 us
    another operation x1, other arithmetic, cell_block(): cumul = jnp.cumsum(forget, axis=-1)  2.75 us
  transfers between devices with their start and end apart: 2, of which 2 were waited for; matrix products, arithmetic and copies ran while one was open for 1% of the time, Pallas kernels for 0%

profile of v1, /device:TPU:0, one launch (start us, length us, event | category | flops | bytes accessed | tf_op | source)
XLA Modules:
  0.0 130.2 jit_solution(9464848634471605944)
XLA Ops:
  0.7 0.8 add.114
  1.5 0.7 iota_compare_fusion
  2.2 0.7 bitcast_convert_fusion
  2.9 0.8 copy.77
  3.6 1.4 %fusion.7 = f32[16,4]{1,0:T(8,128)S(1)} fusion(bf16[16,4,4096]{2,1,0:T(4,128)(2,1)} %param.17), kind=kLoop, calls=%fused_computation.16 | loop fusion | flops 786368 | bytes 524544 | tf_op jit(solution)/shard_map/reduce_sum | solution.py:105
  5.0 0.7 convert_element_type.41
  5.7 0.7 fusion.41
  6.5 0.1 copy.93
  6.6 0.1 copy.76
  6.7 1.4 %fusion.9 = bf16[16,4,4096]{2,1,0:T(4,128)(2,1)S(1)} fusion(bf16[16,4,4096]{2,1,0:T(4,128)(2,1)} %param.17, f32[4096]{0:T(1024)S(1)} %convert_element_type.41, f32[16,4]{1,0:T(8,128)S(1)} %add_rsqrt_fusion), kind=kLoop, calls=%fused_computation.18 | loop fusion | flops 1048576 | bytes 1065216 | tf_op jit(solution)/shard_map/convert_element_type | solution.py:106
  8.1 0.1 reshape.103
  8.2 0.3 convolution_add_fusion
  8.5 0.1 reshape.104
  8.6 0.1 reshape.105
  8.7 0.1 fusion.24
  8.8 0.1 fusion.39
  8.9 2.8 %reduce_window_sum.18 = f32[16,4,4]{2,1,0:T(4,128)S(1)} reduce-window(f32[16,4,4]{2,1,0:T(4,128)S(1)} %get-tuple-element.26, f32[]{:T(128)} %constant.13.clone.1), window={size=1x1x4 pad=0_0x0_0x3_0}, to_apply=%region_3.4 | reduce-window | flops 768 | bytes 2052 | tf_op jit(solution)/shard_map/jit(cumsum)/reduce_window_sum | solution.py:36
  11.7 2.7 %reduce_window_sum.17 = f32[16,4,4]{2,1,0:T(4,128)S(1)} reduce-window(f32[16,4,4]{2,1,0:T(4,128)S(1)} %fusion.24, f32[]{:T(128)} %constant.13.clone.1), window={size=1x1x4 pad=0_0x0_0x3_0}, to_apply=%region_1.2 | reduce-window | flops 768 | bytes 2052 | tf_op jit(solution)/shard_map/jit(cumsum)/reduce_window_sum | solution.py:52
  14.4 3.0 %convolution_convert_fusion.1 = bf16[64,512]{1,0:T(8,128)(2,1)S(1)} fusion(bf16[64,4096]{1,0:T(8,128)(2,1)S(1)} %reshape.103, bf16[4096,512]{1,0:T(8,128)(2,1)} %param.21), kind=kOutput, calls=%fused_computation.12 | convolution fusion | flops 268468224 | bytes 4784128 | tf_op jit(solution)/shard_map/dot_general | solution.py:110
  17.5 3.1 %convolution_convert_fusion.2 = bf16[64,512]{1,0:T(8,128)(2,1)S(1)} fusion(bf16[64,4096]{1,0:T(8,128)(2,1)S(1)} %reshape.103, bf16[4096,512]{1,0:T(8,128)(2,1)} %param.20), kind=kOutput, calls=%fused_computation.13 | convolution fusion | flops 268468224 | bytes 4784128 | tf_op jit(solution)/shard_map/dot_general | solution.py:110
  20.6 3.1 %convolution_convert_fusion.3 = bf16[64,512]{1,0:T(8,128)(2,1)S(1)} fusion(bf16[64,4096]{1,0:T(8,128)(2,1)S(1)} %reshape.103, bf16[4096,512]{1,0:T(8,128)(2,1)} %param.19), kind=kOutput, calls=%fused_computation.14 | convolution fusion | flops 268468224 | bytes 4784128 | tf_op jit(solution)/shard_map/dot_general | solution.py:110
  23.7 0.2 fusion.38
  23.9 0.2 fusion.16
  24.1 0.1 subtract_exponential_fusion.1
  24.2 0.6 fusion.13
  24.9 0.1 multiply_add_fusion.1
  25.0 0.3 fusion.22
  25.3 0.5 fusion.42
  25.8 0.1 exponential_maximum_fusion
  25.9 0.1 fusion.29
  26.0 9.1 %multiply_add_fusion = f32[16,4,128,128]{3,2,1,0:T(8,128)S(1)} fusion(f32[16,4,128,128]{3,2,1,0:T(8,128)} %param.27, f32[16,4]{1,0:T(8,128)S(1)} %get-tuple-element.23, bf16[16,4,4,128]{3,2,1,0:T(4,128)(2,1)S(1)} %copy-done.4, bf16[16,4,4,128]{3,2,1,0:T(4,128)(2,1)S(1)} %copy-done.5, f32[16,4,4]{2,1,0:T(4,128)S(1)} %get-tuple-element.33), kind=kOutput, calls=%fused_computation | convolution fusion | flops 52559872 | bytes 8520960 | tf_op jit(solution)/shard_map/bhs,bhsv,bhsd->bhvd/dot_general | solution.py:41
  35.2 3.3 %fusion.23 = f32[16,4,4,128]{3,2,1,0:T(4,128)S(1)} fusion(f32[16,4,128,128]{3,2,1,0:T(8,128)S(1)} %multiply_add_fusion, bf16[16,4,4,128]{3,2,1,0:T(4,128)(2,1)S(1)} %reshape.106), kind=kOutput, calls=%fused_computation.44 | convolution fusion | flops 50331648 | bytes 4390912 | tf_op jit(solution)/shard_map/bhvd,bhtd->bhtv/dot_general | solution.py:63
  38.5 0.6 fusion.17
  39.2 0.3 multiply_multiply_fusion
  39.5 0.9 fusion.6
  40.4 0.2 broadcast_in_dim.52
  40.6 36.7 %all_to_all.5 = bf16[32,64,512]{2,1,0:T(8,128)(2,1)S(1)} all-to-all(bf16[32,64,512]{2,1,0:T(8,128)(2,1)S(1)} %broadcast_in_dim.52), channel_id=1, replica_groups=mesh['kv'=32,'tp'=4] {'kv'}, dimensions={0} | all-to-all | bytes 4194304 | tf_op jit(solution)/shard_map/all_to_all | solution.py:18
  77.3 0.7 fusion.43
  78.0 1.6 %collective-permute-start = (f32[2048,128]{1,0:T(8,128)S(1)}, f32[2048,128]{1,0:T(8,128)S(1)}, u32[]{:S(2)}, u32[]{:S(2)}) collective-permute-start(f32[2048,128]{1,0:T(8,128)S(1)} %fusion.43), channel_id=1, source_target_pairs={{0,1},{1,0},{2,3},{3,2},{4,5},{5,4},{6,7},{7,6},{8,9},{9,8},{10,11... | collective-permute-start | bytes 3145736 | tf_op jit(solution)/shard_map/ppermute | solution.py:149
  79.6 23.7 %collective-permute-done = f32[2048,128]{1,0:T(8,128)S(1)} collective-permute-done((f32[2048,128]{1,0:T(8,128)S(1)}, f32[2048,128]{1,0:T(8,128)S(1)}, u32[]{:S(2)}, u32[]{:S(2)}) %collective-permute-start) | collective-permute-done | bytes 1048608 | tf_op jit(solution)/shard_map/ppermute | solution.py:149
  103.3 0.1 add.137
  103.4 3.1 %collective-permute-start.1 = (f32[2048,128]{1,0:T(8,128)S(1)}, f32[2048,128]{1,0:T(8,128)S(1)}, u32[]{:S(2)}, u32[]{:S(2)}) collective-permute-start(f32[2048,128]{1,0:T(8,128)S(1)} %add.137), channel_id=1, source_target_pairs={{0,2},{1,3},{2,0},{3,1},{4,6},{5,7},{6,4},{7,5},{8,10},{9,11},{10,... | collective-permute-start | bytes 3145736 | tf_op jit(solution)/shard_map/ppermute | solution.py:149
  106.5 0.7 copy.87
  107.2 0.1 copy.85
  107.3 0.1 copy.86
  107.4 0.6 pad_maximum_fusion
  108.0 21.3 %collective-permute-done.1 = f32[2048,128]{1,0:T(8,128)S(1)} collective-permute-done((f32[2048,128]{1,0:T(8,128)S(1)}, f32[2048,128]{1,0:T(8,128)S(1)}, u32[]{:S(2)}, u32[]{:S(2)}) %collective-permute-start.1) | collective-permute-done | bytes 1048608 | tf_op jit(solution)/shard_map/ppermute | solution.py:149
  129.3 0.9 add_convert_fusion
  (32 shorter events, 0.3 us)
Async XLA Ops:
  0.6 7.6 %copy-start = (bf16[4096,32]{0,1:T(8,128)(2,1)S(1)}, bf16[4096,32]{0,1:T(8,128)(2,1)}, u32[]{:S(2)}) copy-start(bf16[4096,32]{0,1:T(8,128)(2,1)} %param.23) | copy-start | bytes 786436
  17.5 6.7 %copy-start.4 = (bf16[16,4,4,128]{3,2,1,0:T(4,128)(2,1)S(1)}, bf16[16,4,4,128]{3,2,1,0:T(4,128)(2,1)}, u32[]{:S(2)}) copy-start(bf16[16,4,4,128]{3,2,1,0:T(4,128)(2,1)} %param.30) | copy-start | bytes 196612
  20.6 4.3 %copy-start.8 = (f32[16,4,128]{2,1,0:T(4,128)S(1)}, f32[16,4,128]{2,1,0:T(4,128)}, u32[]{:S(2)}) copy-start(f32[16,4,128]{2,1,0:T(4,128)} %param.28) | copy-start | bytes 98308
  20.6 5.4 %copy-start.5 = (bf16[16,4,4,128]{3,2,1,0:T(4,128)(2,1)S(1)}, bf16[16,4,4,128]{3,2,1,0:T(4,128)(2,1)}, u32[]{:S(2)}) copy-start(bf16[16,4,4,128]{3,2,1,0:T(4,128)(2,1)} %param.31) | copy-start | bytes 196612
  24.9 10.3 %copy-start.7 = (bf16[16,4,4,128]{3,2,1,0:T(4,128)(2,1)}, bf16[16,4,4,128]{3,2,1,0:T(4,128)(2,1)S(1)}, u32[]{:S(2)}) copy-start(bf16[16,4,4,128]{3,2,1,0:T(4,128)(2,1)S(1)} %get-tuple-element.40) | copy-start | bytes 196612
  24.9 13.7 %copy-start.6 = (bf16[16,4,4,128]{3,2,1,0:T(4,128)(2,1)}, bf16[16,4,4,128]{3,2,1,0:T(4,128)(2,1)S(1)}, u32[]{:S(2)}) copy-start(bf16[16,4,4,128]{3,2,1,0:T(4,128)(2,1)S(1)} %get-tuple-element.39) | copy-start | bytes 196612
  25.0 10.2 %copy-start.9 = (f32[16,4,128]{2,1,0:T(4,128)}, f32[16,4,128]{2,1,0:T(4,128)S(1)}, u32[]{:S(2)}) copy-start(f32[16,4,128]{2,1,0:T(4,128)S(1)} %multiply_add_fusion.1) | copy-start | bytes 98308
  35.1 5.2 %copy-start.1 = (f32[16,4,128,128]{3,2,1,0:T(8,128)}, f32[16,4,128,128]{3,2,1,0:T(8,128)S(1)}, u32[]{:S(2)}) copy-start(f32[16,4,128,128]{3,2,1,0:T(8,128)S(1)} %multiply_add_fusion) | copy-start | bytes 12582916
  35.2 4.3 %copy-start.2 = (bf16[4096,512]{1,0:T(8,128)(2,1)S(1)}, bf16[4096,512]{1,0:T(8,128)(2,1)}, u32[]{:S(2)}) copy-start(bf16[4096,512]{1,0:T(8,128)(2,1)} %param.22) | copy-start | bytes 12582916
  40.4 36.9 %copy-start.3 = (bf16[512,128]{1,0:T(8,128)(2,1)S(1)}, bf16[512,128]{1,0:T(8,128)(2,1)}, u32[]{:S(2)}) copy-start(bf16[512,128]{1,0:T(8,128)(2,1)} %param.26) | copy-start | bytes 393220
  78.0 25.3 %collective-permute-start = (f32[2048,128]{1,0:T(8,128)S(1)}, f32[2048,128]{1,0:T(8,128)S(1)}, u32[]{:S(2)}, u32[]{:S(2)}) collective-permute-start(f32[2048,128]{1,0:T(8,128)S(1)} %fusion.43), channel_id=1, source_target_pairs={{0,1},{1,0},{2,3},{3,2},{4,5},{5,4},{6,7},{7,6},{8,9},{9,8},{10,11... | collective-permute-start | bytes 3145736 | tf_op jit(solution)/shard_map/ppermute | solution.py:149
  103.4 25.9 %collective-permute-start.1 = (f32[2048,128]{1,0:T(8,128)S(1)}, f32[2048,128]{1,0:T(8,128)S(1)}, u32[]{:S(2)}, u32[]{:S(2)}) collective-permute-start(f32[2048,128]{1,0:T(8,128)S(1)} %add.137), channel_id=1, source_target_pairs={{0,2},{1,3},{2,0},{3,1},{4,6},{5,7},{6,4},{7,5},{8,10},{9,11},{10,... | collective-permute-start | bytes 3145736 | tf_op jit(solution)/shard_map/ppermute | solution.py:149
